TPU v7x, 32 devices: a whole 2x2x4 slice. The times are simulated.
32 devices in a mesh: ra: 4 (over z), cb: 4 (over y, x), dp: 2 (over core).
Axes of the slice: x: 2, y: 2, z: 4, core: 2. Of those that a mesh axis runs over, the one named last changes fastest.
Arguments:
- stream: bfloat16 [4, 64, 4096], P('dp', None, 'ra'), may hold values from -16 to 16
- norm_gain: bfloat16 [2, 4096], P(None, 'ra'), may hold values from 0.099609375 to 1.8984375
- gate_weight: bfloat16 [2, 4096, 12288], P(None, 'ra', 'cb'), may hold values from -0.09375 to 0.09375
- value_weight: bfloat16 [2, 4096, 12288], P(None, 'ra', 'cb'), may hold values from -0.09375 to 0.09375
- gate_taps: bfloat16 [2, 3, 12288], P(None, None, 'cb'), may hold values from -3 to 3
- value_taps: bfloat16 [2, 3, 12288], P(None, None, 'cb'), may hold values from -3 to 3
- gate_bias: bfloat16 [2, 12288], P(None, 'cb'), may hold values from -3 to 3
- value_bias: bfloat16 [2, 12288], P(None, 'cb'), may hold values from -3 to 3
- down_weight: bfloat16 [2, 12288, 4096], P(None, 'cb', 'ra'), may hold values from -0.0546875 to 0.0546875
- final_gain: bfloat16 [4096], P('ra'), may hold values from 0.099609375 to 1.8984375
Outputs:
- mixed: bfloat16 [4, 64, 4096], P('dp', None, 'ra')
All inputs are finite; a program needn't handle non-finite values.
Results may differ from a plain program's by a relative error of at most 0.035.
Values may be sent and summed in bfloat16 or wider, within the bound.
A program may use at most 128 MiB of HBM per device.

v0:
```python
import jax
import jax.numpy as jnp
from jax import lax
from jax.sharding import PartitionSpec as P

D = 4096
LAYERS = 2


EPS = 1e-06


def rms_scaled(stream_in, gain_row):
    values = stream_in.astype(jnp.float32)
    squares = lax.psum(jnp.sum(values * values, axis=-1, keepdims=True), "ra")
    return values * lax.rsqrt(squares / D + EPS) * gain_row.astype(jnp.float32)


def causal_mix(up_rows, taps, bias):
    length = up_rows.shape[1]
    count = taps.shape[0]
    padded = jnp.pad(up_rows.astype(jnp.float32), ((0, 0), (count - 1, 0), (0, 0)))
    result = jnp.zeros(up_rows.shape, jnp.float32) + bias.astype(jnp.float32)
    for tap_index in range(count):
        result = result + padded[:, tap_index : tap_index + length] * taps[tap_index].astype(
            jnp.float32
        )
    return result


def body(
    stream,
    norm_gain,
    gate_weight,
    value_weight,
    gate_taps,
    value_taps,
    gate_bias,
    value_bias,
    down_weight,
    final_gain,
):
    batch_rows, length, width = stream.shape
    ff_local = gate_weight.shape[2]
    current = stream
    for layer_index in range(LAYERS):
        normed = rms_scaled(current, norm_gain[layer_index]).astype(jnp.bfloat16).reshape(-1, width)
        gate_partial = jnp.dot(
            normed, gate_weight[layer_index], preferred_element_type=jnp.float32
        ).reshape(batch_rows, length, ff_local)
        value_partial = jnp.dot(
            normed, value_weight[layer_index], preferred_element_type=jnp.float32
        ).reshape(batch_rows, length, ff_local)
        down_local = down_weight[layer_index]
        gate_sum, value_sum = (
            lax.psum_scatter(
                gate_partial.astype(jnp.bfloat16), "ra", scatter_dimension=2, tiled=True
            ).astype(jnp.float32),
            lax.psum_scatter(
                value_partial.astype(jnp.bfloat16), "ra", scatter_dimension=2, tiled=True
            ).astype(jnp.float32),
        )
        slice_width = gate_sum.shape[2]
        lower = lax.axis_index("ra") * slice_width
        gate_slice = lax.dynamic_slice_in_dim(gate_taps[layer_index], lower, slice_width, 1)
        value_slice = lax.dynamic_slice_in_dim(value_taps[layer_index], lower, slice_width, 1)
        gate_shift = lax.dynamic_slice_in_dim(gate_bias[layer_index], lower, slice_width, 0)
        value_shift = lax.dynamic_slice_in_dim(value_bias[layer_index], lower, slice_width, 0)
        gate_conv = causal_mix(gate_sum.astype(jnp.bfloat16), gate_slice, gate_shift)
        value_conv = causal_mix(value_sum.astype(jnp.bfloat16), value_slice, value_shift)
        hidden = (jax.nn.gelu(gate_conv) * value_conv).astype(jnp.bfloat16)
        block_rows = lax.all_gather(hidden, "ra", axis=2, tiled=True)
        count = block_rows.shape[2]
        term = jnp.dot(
            block_rows.reshape(-1, count), down_local, preferred_element_type=jnp.float32
        )
        branch = lax.psum(term.astype(jnp.bfloat16), "cb").astype(jnp.float32)
        current = (
            0.5 * current.astype(jnp.float32) + branch.reshape(batch_rows, length, width)
        ).astype(jnp.bfloat16)
    return rms_scaled(current, final_gain).astype(jnp.bfloat16)


def solution(mesh):
    in_specs = (
        P("dp", None, "ra"),
        P(None, "ra"),
        P(None, "ra", "cb"),
        P(None, "ra", "cb"),
        P(None, None, "cb"),
        P(None, None, "cb"),
        P(None, "cb"),
        P(None, "cb"),
        P(None, "cb", "ra"),
        P("ra"),
    )
    out_specs = P("dp", None, "ra")
    return jax.shard_map(body, mesh=mesh, in_specs=in_specs, out_specs=out_specs, check_vma=False)
```

profile of v0, /device:TPU:0, one launch (start us, length us, event | category | flops | bytes accessed | tf_op | source)
XLA Modules:
  0.0 290.6 jit_solution(2010544804384724141)
XLA Ops:
  6.5 1.1 fusion.41
  7.6 13.5 %psum.35 = f32[2,64,1]{1,0,2:T(2,128)S(1)} all-reduce(f32[2,64,1]{1,0,2:T(2,128)S(1)} %bitcast.56), channel_id=1, replica_groups=mesh['ra'=4,'cb'=4,'dp'=2] {'ra'}, use_global_device_ids=true, to_apply=%region_1.0 | all-reduce | flops 128 | bytes 1024 | tf_op jit(solution)/shard_map/psum | solution.py:15
  21.9 4.8 %fusion.21 = bf16[2,64,3072]{2,1,0:T(8,128)(2,1)} fusion(bf16[2,1024,3072]{2,1,0:T(8,128)(2,1)} %param.13, bf16[2,64,1024]{2,1,0:T(8,128)(2,1)} %param.10, f32[1024]{0:T(1024)S(1)} %bitcast.60, f32[2,64]{1,0:T(2,128)S(1)} %rsqrt_bitcast_fusion.2), kind=kOutput, calls=%fused_computation.19 | convolution fusion | flops 806223872 | bytes 7344640 | tf_op jit(solution)/shard_map/dot_general | solution.py:51
  26.9 4.7 %fusion.18 = bf16[2,64,3072]{2,1,0:T(8,128)(2,1)} fusion(bf16[2,1024,3072]{2,1,0:T(8,128)(2,1)} %param.12, bf16[2,64,1024]{2,1,0:T(8,128)(2,1)S(1)} %copy-done, f32[1024]{0:T(1024)S(1)} %bitcast.61, f32[2,64]{1,0:T(2,128)S(1)} %rsqrt_bitcast_fusion.2), kind=kOutput, calls=%fused_computation.18 | convolution fusion | flops 806223872 | bytes 7344640 | tf_op jit(solution)/shard_map/dot_general | solution.py:48
  32.0 16.3 %reduce-scatter.7.cloned.1.call-done = bf16[2,64,768]{2,1,0:T(8,128)(2,1)} async-done(((bf16[2,64,3072]{2,1,0:T(8,128)(2,1)}), bf16[2,64,768]{2,1,0:T(8,128)(2,1)}) %reduce-scatter.7.cloned.1.call-update) | async-done | bytes 196624 | tf_op jit(solution)/shard_map/reduce_scatter | solution.py:59
  48.3 1.0 convert_element_type.175
  49.2 24.0 %reduce-scatter.5.cloned.1.call-done = bf16[2,64,768]{2,1,0:T(8,128)(2,1)} async-done(((bf16[2,64,3072]{2,1,0:T(8,128)(2,1)}), bf16[2,64,768]{2,1,0:T(8,128)(2,1)}) %reduce-scatter.5.cloned.1.call-update) | async-done | bytes 196624 | tf_op jit(solution)/shard_map/reduce_scatter | solution.py:56
  74.6 17.9 %all_gather.6 = bf16[2,64,3072]{2,1,0:T(8,128)(2,1)S(1)} all-gather(bf16[2,64,768]{2,1,0:T(8,128)(2,1)S(1)} %fusion.59), channel_id=1, replica_groups=mesh['ra'=4,'cb'=4,'dp'=2] {'ra'}, dimensions={2}, use_global_device_ids=true | all-gather | bytes 983040 | tf_op jit(solution)/shard_map/all_gather | solution.py:72
  92.5 4.5 %fusion.30 = bf16[128,1024]{1,0:T(8,128)(2,1)} fusion(bf16[128,3072]{1,0:T(8,128)(2,1)S(1)} %bitcast.51, bf16[2,3072,1024]{2,1,0:T(8,128)(2,1)} %param.18), kind=kOutput, calls=%fused_computation.22 | convolution fusion | flops 805437440 | bytes 7340032 | tf_op jit(solution)/shard_map/dot_general | solution.py:74
  97.1 42.6 %all-reduce.7.cloned.1.call-done = bf16[2,64,1024]{2,1,0:T(8,128)(2,1)} async-done(((bf16[2,64,1024]{2,1,0:T(8,128)(2,1)}), bf16[2,64,1024]{2,1,0:T(8,128)(2,1)}) %all-reduce.7.cloned.1.call-update) | async-done | bytes 262160 | tf_op jit(solution)/shard_map/psum | solution.py:77
  139.8 1.1 fusion.46
  140.9 11.7 %psum.37 = f32[2,64,1]{1,0,2:T(2,128)S(1)} all-reduce(f32[2,64,1]{1,0,2:T(2,128)S(1)} %bitcast.55), channel_id=1, replica_groups=mesh['ra'=4,'cb'=4,'dp'=2] {'ra'}, use_global_device_ids=true, to_apply=%region_6.7 | all-reduce | flops 128 | bytes 1024 | tf_op jit(solution)/shard_map/psum | solution.py:15
  152.6 4.7 %fusion.27 = bf16[2,64,3072]{2,1,0:T(8,128)(2,1)} fusion(bf16[2,1024,3072]{2,1,0:T(8,128)(2,1)} %param.13, bf16[2,64,1024]{2,1,0:T(8,128)(2,1)S(1)} %get-tuple-element.18, f32[1024]{0:T(1024)S(1)} %bitcast.58, f32[2,64]{1,0:T(2,128)S(1)} %rsqrt_bitcast_fusion.1), kind=kOutput, calls=%fused_computation.21 | convolution fusion | flops 806223872 | bytes 7344640 | tf_op jit(solution)/shard_map/dot_general | solution.py:51
  157.4 4.7 %fusion.24 = bf16[2,64,3072]{2,1,0:T(8,128)(2,1)} fusion(bf16[2,1024,3072]{2,1,0:T(8,128)(2,1)} %param.12, bf16[2,64,1024]{2,1,0:T(8,128)(2,1)S(1)} %get-tuple-element.18, f32[1024]{0:T(1024)S(1)} %bitcast.59, f32[2,64]{1,0:T(2,128)S(1)} %rsqrt_bitcast_fusion.1), kind=kOutput, calls=%fused_computation.20 | convolution fusion | flops 806223872 | bytes 7344640 | tf_op jit(solution)/shard_map/dot_general | solution.py:48
  162.3 15.6 %reduce-scatter.11.cloned.1.call-done = bf16[2,64,768]{2,1,0:T(8,128)(2,1)} async-done(((bf16[2,64,3072]{2,1,0:T(8,128)(2,1)}), bf16[2,64,768]{2,1,0:T(8,128)(2,1)}) %reduce-scatter.11.cloned.1.call-update) | async-done | bytes 196624 | tf_op jit(solution)/shard_map/reduce_scatter | solution.py:59
  177.9 1.0 convert_element_type.190
  178.8 23.9 %reduce-scatter.9.cloned.1.call-done = bf16[2,64,768]{2,1,0:T(8,128)(2,1)} async-done(((bf16[2,64,3072]{2,1,0:T(8,128)(2,1)}), bf16[2,64,768]{2,1,0:T(8,128)(2,1)}) %reduce-scatter.9.cloned.1.call-update) | async-done | bytes 196624 | tf_op jit(solution)/shard_map/reduce_scatter | solution.py:56
  202.7 1.0 convert_element_type.186
  204.1 17.9 %all_gather.7 = bf16[2,64,3072]{2,1,0:T(8,128)(2,1)S(1)} all-gather(bf16[2,64,768]{2,1,0:T(8,128)(2,1)S(1)} %fusion.71), channel_id=1, replica_groups=mesh['ra'=4,'cb'=4,'dp'=2] {'ra'}, dimensions={2}, use_global_device_ids=true | all-gather | bytes 983040 | tf_op jit(solution)/shard_map/all_gather | solution.py:72
  222.0 4.5 %fusion.33 = bf16[128,1024]{1,0:T(8,128)(2,1)} fusion(bf16[128,3072]{1,0:T(8,128)(2,1)S(1)} %bitcast.52, bf16[2,3072,1024]{2,1,0:T(8,128)(2,1)} %param.18), kind=kOutput, calls=%fused_computation.23 | convolution fusion | flops 805437440 | bytes 7340032 | tf_op jit(solution)/shard_map/dot_general | solution.py:74
  226.6 42.6 %all-reduce.9.cloned.1.call-done = bf16[2,64,1024]{2,1,0:T(8,128)(2,1)} async-done(((bf16[2,64,1024]{2,1,0:T(8,128)(2,1)}), bf16[2,64,1024]{2,1,0:T(8,128)(2,1)}) %all-reduce.9.cloned.1.call-update) | async-done | bytes 262160 | tf_op jit(solution)/shard_map/psum | solution.py:77
  269.2 1.1 fusion.36
  270.3 11.7 %psum.39 = f32[2,64,1]{1,0,2:T(2,128)S(1)} all-reduce(f32[2,64,1]{1,0,2:T(2,128)S(1)} %bitcast.57), channel_id=1, replica_groups=mesh['ra'=4,'cb'=4,'dp'=2] {'ra'}, use_global_device_ids=true, to_apply=%region_11.12 | all-reduce | flops 128 | bytes 1024 | tf_op jit(solution)/shard_map/psum | solution.py:15
  282.0 1.8 fusion.38
  (40 shorter events, 3.2 us)
Async XLA Ops:
  6.5 41.8 %reduce-scatter.7.cloned.1.call-start = ((), (), s32[]{:S(2)}) async-start(), calls=%async_computation.5 | async-start | bytes 983040 | tf_op jit(solution)/shard_map/reduce_scatter | solution.py:59
  21.9 5.0 %copy-start = (bf16[2,64,1024]{2,1,0:T(8,128)(2,1)S(1)}, bf16[2,64,1024]{2,1,0:T(8,128)(2,1)}, u32[]{:S(2)}) copy-start(bf16[2,64,1024]{2,1,0:T(8,128)(2,1)} %param.10) | copy-start | bytes 786436
  26.8 4.9 %copy-start.3 = (bf16[2,3072]{1,0:T(2,128)(2,1)S(1)}, bf16[2,3072]{1,0:T(2,128)(2,1)}, u32[]{:S(2)}) copy-start(bf16[2,3072]{1,0:T(2,128)(2,1)} %param.16) | copy-start | bytes 36868
  26.8 5.0 %copy-start.4 = (bf16[2,3072]{1,0:T(2,128)(2,1)S(1)}, bf16[2,3072]{1,0:T(2,128)(2,1)}, u32[]{:S(2)}) copy-start(bf16[2,3072]{1,0:T(2,128)(2,1)} %param.17) | copy-start | bytes 36868
  26.8 5.0 %copy-start.1 = (bf16[2,3,3072]{2,0,1:T(2,128)(2,1)S(1)}, bf16[2,3,3072]{2,0,1:T(2,128)(2,1)}, u32[]{:S(2)}) copy-start(bf16[2,3,3072]{2,0,1:T(2,128)(2,1)} %param.14) | copy-start | bytes 110596
  26.8 5.1 %copy-start.2 = (bf16[2,3,3072]{2,0,1:T(2,128)(2,1)S(1)}, bf16[2,3,3072]{2,0,1:T(2,128)(2,1)}, u32[]{:S(2)}) copy-start(bf16[2,3,3072]{2,0,1:T(2,128)(2,1)} %param.15) | copy-start | bytes 110596
  26.8 46.5 %reduce-scatter.5.cloned.1.call-start = ((), (), s32[]{:S(2)}) async-start(), calls=%async_computation.4 | async-start | bytes 983040 | tf_op jit(solution)/shard_map/reduce_scatter | solution.py:56
  31.6 108.1 %all-reduce.7.cloned.1.call-start = ((), (), s32[]{:S(2)}) async-start(), calls=%async_computation.6 | async-start | bytes 524288 | tf_op jit(solution)/shard_map/psum | solution.py:77
  97.1 80.8 %reduce-scatter.11.cloned.1.call-start = ((), (), s32[]{:S(2)}) async-start(), calls=%async_computation.8 | async-start | bytes 983040 | tf_op jit(solution)/shard_map/reduce_scatter | solution.py:59
  157.3 45.4 %reduce-scatter.9.cloned.1.call-start = ((), (), s32[]{:S(2)}) async-start(), calls=%async_computation.7 | async-start | bytes 983040 | tf_op jit(solution)/shard_map/reduce_scatter | solution.py:56
  162.1 107.1 %all-reduce.9.cloned.1.call-start = ((), (), s32[]{:S(2)}) async-start(), calls=%async_computation.9 | async-start | bytes 524288 | tf_op jit(solution)/shard_map/psum | solution.py:77
  178.8 47.7 %copy-start.5 = (bf16[1024]{0:T(1024)(128)(2,1)S(1)}, bf16[1024]{0:T(1024)(128)(2,1)}, u32[]{:S(2)}) copy-start(bf16[1024]{0:T(1024)(128)(2,1)} %param.19) | copy-start | bytes 6148
Sparse Core Ops, SparseCore 0:
  26.9 21.3 reduce-scatter.6
  50.6 22.6 reduce-scatter.4
  97.2 42.4 all-reduce.6
  157.4 20.3 reduce-scatter.10
  180.0 22.6 reduce-scatter.8
  226.7 42.4 all-reduce.8
where the time goes:
time: 291 us
  waiting for transfers between devices  165 us (57%)
  blocking collectives  72.6 us (25%)
  matrix products  28.1 us (10%)
  between operations  13.7 us (5%)
  other arithmetic  10.7 us (4%)
    psum x2, waiting for transfers between devices, body(): branch = lax.psum(term.astype(jnp.bfloat16), 'cb').astype(jnp.float32)  85.2 us
    reduce_scatter x2, waiting for transfers between devices, body(): lax.psum_scatter(gate_partial.astype(jnp.bfloat16), 'ra', scatter_dimensi...  47.9 us
    psum x3, blocking collectives, rms_scaled(): squares = lax.psum(jnp.sum(values * values, axis=-1, keepdims=True), 'ra')  36.8 us
    all_gather x2, blocking collectives, body(): block_rows = lax.all_gather(hidden, 'ra', axis=2, tiled=True)  35.8 us
    reduce_scatter x2, waiting for transfers between devices, body(): lax.psum_scatter(value_partial.astype(jnp.bfloat16), 'ra', scatter_dimens...  31.8 us
    dot_general x2, matrix products, body(): jnp.dot(normed, value_weight[layer_index], preferred_element_type=jnp.flo...  9.57 us
    dot_general x2, matrix products, body(): jnp.dot(normed, gate_weight[layer_index], preferred_element_type=jnp.floa...  9.49 us
    dot_general x2, matrix products, body(): jnp.dot(block_rows.reshape(-1, count), down_local, preferred_element_type...  9.04 us
  transfers between devices with their start and end apart: 6, of which 6 were waited for; matrix products, arithmetic and copies ran while one was open for 4% of the time, Pallas kernels for 0%

commit v1 on v0

v1 whole, which is shorter than its diff:
```python
import functools

import jax
import jax.numpy as jnp
from jax import lax
from jax.experimental import pallas as pl
from jax.experimental.pallas import tpu as pltpu
from jax.sharding import PartitionSpec as P

EPS = 1e-06
MESH = pl.DeviceIdType.MESH
LANES = 128
GROUPS = 2
CHUNKS = 6
SKEW = 2
SKEW_BACK = 2
SKEW_CB = 2


def chain_kernel(
    dims,
    s_in, ng, gt, vt, gb, vb, fg, wg_hbm, wv_hbm, dn_hbm,
    out,
    wg, wv, dn, cur, u, part, rs_send, rs_recv, hid, acc, scale,
    sq_send, sq_recv, tbuf, rbuf, snew,
    wsem, wlate, dsem, rs_ss, rs_rs, ag_ss, ag_rs, sq_ss, sq_rs, t_ss, t_rs, n_ss, n_rs,
):
    n, m, width, length = dims
    layers, dl, ff = wg.shape
    groups, rows, _ = cur.shape
    chunks = part.shape[2]
    cw = ff // 2 // chunks
    rq = rows // m
    me = lax.axis_index("ra")
    mc = lax.axis_index("cb")
    head = SKEW * (n - 1)
    t_term = chunks + head + SKEW_BACK * (n - 1)
    t_own = t_term + SKEW_CB
    t_back = t_own + SKEW_CB
    per_layer = t_back + 1
    lag = per_layer // groups
    f32 = jnp.float32

    def wcopy(d, c, which):
        src, dst = ((wg_hbm, wg), (wv_hbm, wv))[which]
        cols = pl.ds(pl.multiple_of(d * (ff // 2) + c * cw, LANES), cw)
        return pltpu.make_async_copy(src.at[0, :, cols], dst.at[0, :, cols], wsem.at[which, d, c])

    def late(l, which):
        src, dst = ((wg_hbm, wg), (wv_hbm, wv))[which]
        return pltpu.make_async_copy(src.at[l], dst.at[l], wlate.at[which, l])

    def dcopy(l):
        return pltpu.make_async_copy(dn_hbm.at[l], dn.at[l], dsem.at[l])

    for c in range(chunks):
        for d in range(2):
            for which in range(2):
                wcopy(d, c, which).start()

    barrier = pltpu.get_barrier_semaphore()
    for o in range(1, n):
        pl.semaphore_signal(barrier, inc=1, device_id={"ra": lax.rem(me + o, n)}, device_id_type=MESH)
    for o in range(1, m):
        pl.semaphore_signal(barrier, inc=1, device_id={"cb": lax.rem(mc + o, m)}, device_id_type=MESH)
    pl.semaphore_wait(barrier, n + m - 2)

    def remote(src, dst, ss, rs, **to):
        return pltpu.make_async_remote_copy(
            src_ref=src, dst_ref=dst, send_sem=ss, recv_sem=rs, device_id=to, device_id_type=MESH
        )

    def toward(d, back):
        up = (d == 1) != back
        return lax.rem(me + (1 if up else n - 1), n)

    def rs_copy(l, h, d, c):
        return remote(
            rs_send.at[l, h, d, c], rs_recv.at[l, h, d, c], rs_ss.at[l, h, d, c], rs_rs.at[l, h, d, c],
            ra=toward(d, False),
        )

    def ag_copy(l, h, d, c):
        return remote(
            hid.at[l, h, d, c], hid.at[l, h, d, c], ag_ss.at[l, h, d, c], ag_rs.at[l, h, d, c],
            ra=toward(d, True),
        )

    def sq_copy(l, h, o):
        return remote(
            sq_send.at[l, h], sq_recv.at[l, h, o], sq_ss.at[l, h, o], sq_rs.at[l, h, o],
            ra=lax.rem(me + o, n),
        )

    def t_copy(l, h, o):
        to = lax.rem(mc + o, m)
        return remote(
            tbuf.at[l, h, pl.ds(pl.multiple_of(to * rq, rq), rq)], rbuf.at[l, h, o],
            t_ss.at[l, h, o], t_rs.at[l, h, o], cb=to,
        )

    def own(q):
        return pl.ds(pl.multiple_of(q * rq, rq), rq)

    def n_copy(l, h, o):
        mine = own(mc)
        return remote(
            snew.at[l, h, mine], snew.at[l, h, mine], n_ss.at[l, h, o], n_rs.at[l, h, o],
            cb=lax.rem(mc + o, m),
        )

    def n_wait(l, h, o):
        theirs = own(lax.rem(mc + m - o, m))
        remote(
            snew.at[l, h, theirs], snew.at[l, h, theirs], n_ss.at[l, h, o], n_rs.at[l, h, o],
            cb=lax.rem(mc + o, m),
        ).wait_recv()

    def row_of(ref, l, cols=slice(None)):
        block = ref[:, cols].astype(f32)
        row = block[0:1]
        for i in range(1, layers):
            row = jnp.where(l == i, block[i : i + 1], row)
        return row

    def prep(h, l, s):
        cur[h] = s
        values = s.astype(f32)
        u[h] = (values * row_of(ng, l)).astype(jnp.bfloat16)
        total = jnp.sum(values * values, axis=1, keepdims=True)
        square = jnp.broadcast_to(jnp.concatenate([total] * (LANES // rows), axis=0), (LANES, LANES))
        sq_send[l, h] = square.T[0:8]
        for o in range(1, n):
            sq_copy(l, h, o).start()
        acc[h] = jnp.zeros((rows, dl), f32)

    def finish_scale(h, l):
        total = sq_send[l, h]
        for o in range(1, n):
            sq_copy(l, h, o).wait_recv()
            total = total + sq_recv[l, h, o]
        inverse = lax.rsqrt(total / width + EPS)
        scale[h] = jnp.broadcast_to(inverse[0:1], (LANES, LANES)).T[0:rows]

    def down(h, l, d, c):
        at = pl.ds(pl.multiple_of(d * (ff // 2) + c * cw, LANES), cw)
        acc[h] += jnp.dot(hid[l, h, d, c], dn[l, at, :], preferred_element_type=f32)

    def mix(x, taps, bias):
        position = lax.rem(lax.broadcasted_iota(jnp.int32, x.shape, 0), length)
        count = taps.shape[0]
        result = bias + x * taps[count - 1 : count]
        for back in range(1, count):
            moved = jnp.where(position >= back, pltpu.roll(x, back, 0), 0.0)
            result = result + moved * taps[count - 1 - back : count - back]
        return result

    def hidden(h, l, d, c):
        cols = pl.ds(pl.multiple_of(d * (ff // 2) + c * cw, LANES), cw)
        factor = jnp.concatenate([scale[h]] * (cw // LANES), axis=1)
        gate = (part[h, d, c, :, :cw] + rs_recv[l, h, d, c, :, :cw].astype(f32)) * factor
        value = (part[h, d, c, :, cw:] + rs_recv[l, h, d, c, :, cw:].astype(f32)) * factor
        gate = mix(gate, gt[l, :, cols].astype(f32), row_of(gb, l, cols))
        value = mix(value, vt[l, :, cols].astype(f32), row_of(vb, l, cols))
        hid[l, h, d, c] = (jax.nn.gelu(gate) * value).astype(jnp.bfloat16)

    def step(h, l, tau):
        @pl.when(tau < chunks)
        def _():
            for d in range(2):
                if h == 0:

                    @pl.when(l == 0)
                    def _():
                        wcopy(d, tau, 0).wait()
                        wcopy(d, tau, 1).wait()

                    if d == 0:

                        @pl.when((l > 0) & (tau == 0))
                        def _():
                            late(l, 0).wait()
                            late(l, 1).wait()

                cols = pl.ds(pl.multiple_of(d * (ff // 2) + tau * cw, LANES), cw)
                part[h, d, tau, :, :cw] = jnp.dot(u[h], wg[l, :, cols], preferred_element_type=f32)
                part[h, d, tau, :, cw:] = jnp.dot(u[h], wv[l, :, cols], preferred_element_type=f32)

        @pl.when(tau == head)
        def _():
            finish_scale(h, l)
            if h == 0:
                dcopy(l).wait()

        for d in range(2):
            k = me if d == 1 else n - 1 - me
            c = tau - SKEW * k

            @pl.when((c >= 0) & (c < chunks))
            def _():
                @pl.when(k == 0)
                def _():
                    rs_send[l, h, d, c] = part[h, d, c].astype(jnp.bfloat16)
                    rs_copy(l, h, d, c).start()

                @pl.when((k > 0) & (k < n - 1))
                def _():
                    rs_copy(l, h, d, c).wait_recv()
                    rs_send[l, h, d, c] = (part[h, d, c] + rs_recv[l, h, d, c].astype(f32)).astype(jnp.bfloat16)
                    rs_copy(l, h, d, c).start()

                @pl.when(k == n - 1)
                def _():
                    rs_copy(l, h, d, c).wait_recv()
                    hidden(h, l, d, c)
                    ag_copy(l, h, d, c).start()
                    down(h, l, d, c)

        for d in range(2):
            j = n - 1 - me if d == 1 else me
            c = tau - head - SKEW_BACK * j

            @pl.when((j > 0) & (c >= 0) & (c < chunks))
            def _():
                ag_copy(l, h, d, c).wait_recv()

                @pl.when(j < n - 1)
                def _():
                    ag_copy(l, h, d, c).start()

                down(h, l, d, c)

        @pl.when(tau == t_term)
        def _():
            tbuf[l, h] = acc[h].astype(jnp.bfloat16)
            for o in range(1, m):
                t_copy(l, h, o).start()

        @pl.when(tau == t_own)
        def _():
            mine = own(mc)
            total = tbuf[l, h, mine].astype(f32)
            for o in range(1, m):
                t_copy(l, h, o).wait_recv()
                total = total + rbuf[l, h, o].astype(f32)
            snew[l, h, mine] = (0.5 * cur[h, mine].astype(f32) + total).astype(jnp.bfloat16)
            for o in range(1, m):
                n_copy(l, h, o).start()

        @pl.when(tau == t_back)
        def _():
            for o in range(1, m):
                n_wait(l, h, o)
            prep(h, l + 1, snew[l, h])

    for h in range(groups):
        prep(h, 0, s_in[h * rows : (h + 1) * rows])

    def body(t, carry):
        @pl.when(t == chunks - 1)
        def _():
            for l in range(layers):
                dcopy(l).start()
                if l + 1 < layers:
                    late(l + 1, 0).start()
                    late(l + 1, 1).start()

        for h in range(groups):
            at = t - h * lag

            @pl.when((at >= 0) & (at < layers * per_layer))
            def _():
                l = at // per_layer
                step(h, l, at - l * per_layer)

        return carry

    lax.fori_loop(0, layers * per_layer + (groups - 1) * lag, body, 0)

    for h in range(groups):
        finish_scale(h, layers)
        factor = jnp.concatenate([scale[h]] * (dl // LANES), axis=1)
        out[h * rows : (h + 1) * rows] = (
            cur[h].astype(f32) * factor * fg[...].astype(f32)
        ).astype(jnp.bfloat16)

    def drain(i, carry):
        l = i // chunks
        c = i - l * chunks
        for h in range(groups):
            for d in range(2):
                k = me if d == 1 else n - 1 - me

                @pl.when(k < n - 1)
                def _():
                    rs_copy(l, h, d, c).wait_send()

                @pl.when(k > 0)
                def _():
                    ag_copy(l, h, d, c).wait_send()

        return carry

    lax.fori_loop(0, layers * chunks, drain, 0)
    for h in range(groups):
        for l in range(layers):
            for o in range(1, m):
                t_copy(l, h, o).wait_send()
                n_copy(l, h, o).wait_send()
        for l in range(layers + 1):
            for o in range(1, n):
                sq_copy(l, h, o).wait_send()


def body(n, m, width, stream, norm_gain, gate_weight, value_weight, gate_taps, value_taps,
         gate_bias, value_bias, down_weight, final_gain):
    batch, length, dl = stream.shape
    layers, _, ff = gate_weight.shape
    groups = GROUPS if batch % GROUPS == 0 else 1
    rows = batch * length // groups
    chunks = CHUNKS
    cw = ff // 2 // chunks
    bf16, f32 = jnp.bfloat16, jnp.float32
    vmem = pl.BlockSpec(memory_space=pltpu.VMEM)
    hbm = pl.BlockSpec(memory_space=pl.ANY)
    dma = pltpu.SemaphoreType.DMA
    result = pl.pallas_call(
        functools.partial(chain_kernel, (n, m, width, length)),
        out_shape=jax.ShapeDtypeStruct((batch * length, dl), bf16),
        in_specs=[vmem] * 7 + [hbm] * 3,
        out_specs=vmem,
        scratch_shapes=[
            pltpu.VMEM(gate_weight.shape, bf16),
            pltpu.VMEM(value_weight.shape, bf16),
            pltpu.VMEM(down_weight.shape, bf16),
            pltpu.VMEM((groups, rows, dl), bf16),
            pltpu.VMEM((groups, rows, dl), bf16),
            pltpu.VMEM((groups, 2, chunks, rows, 2 * cw), f32),
            pltpu.VMEM((layers, groups, 2, chunks, rows, 2 * cw), bf16),
            pltpu.VMEM((layers, groups, 2, chunks, rows, 2 * cw), bf16),
            pltpu.VMEM((layers, groups, 2, chunks, rows, cw), bf16),
            pltpu.VMEM((groups, rows, dl), f32),
            pltpu.VMEM((groups, rows, LANES), f32),
            pltpu.VMEM((layers + 1, groups, 8, LANES), f32),
            pltpu.VMEM((layers + 1, groups, n, 8, LANES), f32),
            pltpu.VMEM((layers, groups, rows, dl), bf16),
            pltpu.VMEM((layers, groups, m, rows // m, dl), bf16),
            pltpu.VMEM((layers, groups, rows, dl), bf16),
            dma((2, 2, chunks)),
            dma((2, layers)),
            dma((layers,)),
            dma((layers, groups, 2, chunks)),
            dma((layers, groups, 2, chunks)),
            dma((layers, groups, 2, chunks)),
            dma((layers, groups, 2, chunks)),
            dma((layers + 1, groups, n)),
            dma((layers + 1, groups, n)),
            dma((layers, groups, m)),
            dma((layers, groups, m)),
            dma((layers, groups, m)),
            dma((layers, groups, m)),
        ],
        compiler_params=pltpu.CompilerParams(
            collective_id=0, has_side_effects=True, vmem_limit_bytes=66_000_000
        ),
    )(
        stream.reshape(batch * length, dl), norm_gain, gate_taps, value_taps, gate_bias, value_bias,
        final_gain.reshape(1, dl), gate_weight, value_weight, down_weight,
    )
    return result.reshape(batch, length, dl)


def solution(mesh):
    n, m = mesh.shape["ra"], mesh.shape["cb"]

    def run(stream, *rest):
        specs = (
            P("dp", None, "ra"),
            P(None, "ra"),
            P(None, "ra", "cb"),
            P(None, "ra", "cb"),
            P(None, None, "cb"),
            P(None, None, "cb"),
            P(None, "cb"),
            P(None, "cb"),
            P(None, "cb", "ra"),
            P("ra"),
        )
        return jax.shard_map(
            functools.partial(body, n, m, stream.shape[2]),
            mesh=mesh, in_specs=specs, out_specs=P("dp", None, "ra"), check_vma=False,
        )(stream, *rest)

    return run
```

time: 291 us -> 117 us (0.40)
  waiting for transfers between devices: 165 us -> 0 us
  Pallas kernels: 0 us -> 111 us
  blocking collectives: 72.6 us -> 0 us
  matrix products: 28.1 us -> 0 us
  between operations: 13.7 us -> 0.01 us
  other arithmetic: 10.7 us -> 0 us
  local copies, waits for them, and re-layouts: 0.19 us -> 5.75 us
    pallas_call x0 -> x1, Pallas kernels: none -> 111 us  [body(): pl.pallas_call(functools.partial(chain_kernel, (n, m, width, length)), ou...]
    psum x2 -> x0, waiting for transfers between devices: 85.2 us -> none  [body(): branch = lax.psum(term.astype(jnp.bfloat16), 'cb').astype(jnp.float32)]
    reduce_scatter x4 -> x0, waiting for transfers between devices: 79.8 us -> none  [the longest x2 47.9 us: body(): lax.psum_scatter(gate_partial.astype(jnp.bfloat16), 'ra', scatter_dimensi...]
    psum x3 -> x0, blocking collectives: 36.8 us -> none  [rms_scaled(): squares = lax.psum(jnp.sum(values * values, axis=-1, keepdims=True), 'ra')]
    all_gather x2 -> x0, blocking collectives: 35.8 us -> none  [body(): block_rows = lax.all_gather(hidden, 'ra', axis=2, tiled=True)]
    dot_general x6 -> x0, matrix products: 28.1 us -> none  [the longest x2 9.57 us: body(): jnp.dot(normed, value_weight[layer_index], preferred_element_type=jnp.flo...]
    convert_element_type x11 -> x0, other arithmetic: 7.23 us -> none  [the longest x4 3.81 us: causal_mix(): up_rows.astype(jnp.float32)]
    unnamed x12 -> x3, local copies, waits for them, and re-layouts: 0.04 us -> 4.48 us
  transfers between devices with their start and end apart: 6 -> 0, of which waited for: 6 -> 0; matrix products, arithmetic and copies ran while one was open for 4% -> 0% of each run, Pallas kernels for 0% -> 0%
where the time goes in v1:
time: 117 us
  Pallas kernels  111 us (95%)
  local copies, waits for them, and re-layouts  5.75 us (5%)
    pallas_call x1, Pallas kernels, body(): pl.pallas_call(functools.partial(chain_kernel, (n, m, width, length)), ou...  111 us
    unnamed x3, local copies, waits for them, and re-layouts  4.48 us

profile of v1, /device:TPU:0, one launch (start us, length us, event | category | flops | bytes accessed | tf_op | source)
XLA Modules:
  0.0 116.8 jit_solution(9342525029713224604)
XLA Ops:
  0.0 1.3 %reshape.10.fg = bf16[1,1024]{1,0:T(2,128)(2,1)} reshape(bf16[1024]{0:T(1024)(128)(2,1)} %param.19) | data formatting | bytes 4096 | tf_op jit(solution)/shard_map/reshape | solution.py:368
  1.3 1.4 %copy.11.gt = bf16[2,3,3072]{2,1,0:T(4,128)(2,1)} copy(bf16[2,3,3072]{2,0,1:T(2,128)(2,1)} %param.14) | data formatting | bytes 73728 | tf_op args[4]
  2.7 1.4 %copy.12.vt = bf16[2,3,3072]{2,1,0:T(4,128)(2,1)} copy(bf16[2,3,3072]{2,0,1:T(2,128)(2,1)} %param.15) | data formatting | bytes 73728 | tf_op args[5]
  4.1 111.1 %shard_map.100 = bf16[128,1024]{1,0:T(8,128)(2,1)} custom-call(bf16[128,1024]{1,0:T(8,128)(2,1)} %bitcast.3, bf16[2,1024]{1,0:T(2,128)(2,1)} %ng.1, bf16[2,3,3072]{2,1,0:T(4,128)(2,1)} %copy.11.gt, bf16[2,3,3072]{2,1,0:T(4,128)(2,1)} %copy.12.vt, bf16[2,3072]{1,0:T(2,128)(2,1)} %gb.1, bf16[2,3072]{1,0:T(2,128)(2,1)} %vb.1, bf16[1,1024]{1,0:T(2,128)(2,1)} %reshape.10.fg, ...), custom_call_target="tpu_custom_call" | custom-call | tf_op jit(solution)/shard_map/pallas_call | solution.py:327
  115.2 1.7 %copy.14 = bf16[2,64,1024]{2,1,0:T(8,128)(2,1)} copy(bf16[2,64,1024]{2,1,0:T(8,128)(2,1)} %bitcast.2) | data formatting | bytes 524288

commit v2 on v1

--- a/solution.py
+++ b/solution.py
@@ -14,6 +14,7 @@
 CHUNKS = 6
 SKEW = 2
 SKEW_BACK = 2
+LAG = 6
 SKEW_CB = 2
 
 
@@ -38,7 +39,7 @@
     t_own = t_term + SKEW_CB
     t_back = t_own + SKEW_CB
     per_layer = t_back + 1
-    lag = per_layer // groups
+    lag = LAG
     f32 = jnp.float32
 
     def wcopy(d, c, which):
@@ -116,8 +117,8 @@
             cb=lax.rem(mc + o, m),
         ).wait_recv()
 
-    def row_of(ref, l, cols=slice(None)):
-        block = ref[:, cols].astype(f32)
+    def row_of(ref, l, *at):
+        block = ref[at].astype(f32)
         row = block[0:1]
         for i in range(1, layers):
             row = jnp.where(l == i, block[i : i + 1], row)
@@ -126,7 +127,7 @@
     def prep(h, l, s):
         cur[h] = s
         values = s.astype(f32)
-        u[h] = (values * row_of(ng, l)).astype(jnp.bfloat16)
+        u[h] = (values * row_of(ng, l, slice(None), slice(None))).astype(jnp.bfloat16)
         total = jnp.sum(values * values, axis=1, keepdims=True)
         square = jnp.broadcast_to(jnp.concatenate([total] * (LANES // rows), axis=0), (LANES, LANES))
         sq_send[l, h] = square.T[0:8]
@@ -148,11 +149,11 @@
 
     def mix(x, taps, bias):
         position = lax.rem(lax.broadcasted_iota(jnp.int32, x.shape, 0), length)
-        count = taps.shape[0]
-        result = bias + x * taps[count - 1 : count]
+        count = len(taps)
+        result = bias + x * taps[count - 1]
         for back in range(1, count):
             moved = jnp.where(position >= back, pltpu.roll(x, back, 0), 0.0)
-            result = result + moved * taps[count - 1 - back : count - back]
+            result = result + moved * taps[count - 1 - back]
         return result
 
     def hidden(h, l, d, c):
@@ -160,8 +161,8 @@
         factor = jnp.concatenate([scale[h]] * (cw // LANES), axis=1)
         gate = (part[h, d, c, :, :cw] + rs_recv[l, h, d, c, :, :cw].astype(f32)) * factor
         value = (part[h, d, c, :, cw:] + rs_recv[l, h, d, c, :, cw:].astype(f32)) * factor
-        gate = mix(gate, gt[l, :, cols].astype(f32), row_of(gb, l, cols))
-        value = mix(value, vt[l, :, cols].astype(f32), row_of(vb, l, cols))
+        gate = mix(gate, [row_of(gt, l, i, slice(None), cols) for i in range(gt.shape[0])], row_of(gb, l, slice(None), cols))
+        value = mix(value, [row_of(vt, l, i, slice(None), cols) for i in range(vt.shape[0])], row_of(vb, l, slice(None), cols))
         hid[l, h, d, c] = (jax.nn.gelu(gate) * value).astype(jnp.bfloat16)
 
     def step(h, l, tau):
@@ -257,7 +258,7 @@
         prep(h, 0, s_in[h * rows : (h + 1) * rows])
 
     def body(t, carry):
-        @pl.when(t == chunks - 1)
+        @pl.when(t == min(chunks - 1, head))
         def _():
             for l in range(layers):
                 dcopy(l).start()
@@ -281,7 +282,7 @@
         finish_scale(h, layers)
         factor = jnp.concatenate([scale[h]] * (dl // LANES), axis=1)
         out[h * rows : (h + 1) * rows] = (
-            cur[h].astype(f32) * factor * fg[...].astype(f32)
+            cur[h].astype(f32) * factor * fg[...].astype(f32).reshape(1, dl)
         ).astype(jnp.bfloat16)
 
     def drain(i, carry):
@@ -364,8 +365,8 @@
             collective_id=0, has_side_effects=True, vmem_limit_bytes=66_000_000
         ),
     )(
-        stream.reshape(batch * length, dl), norm_gain, gate_taps, value_taps, gate_bias, value_bias,
-        final_gain.reshape(1, dl), gate_weight, value_weight, down_weight,
+        stream.reshape(batch * length, dl), norm_gain, gate_taps.swapaxes(0, 1), value_taps.swapaxes(0, 1), gate_bias, value_bias,
+        final_gain, gate_weight, value_weight, down_weight,
     )
     return result.reshape(batch, length, dl)
 

time: 117 us -> 107 us (0.915)
  Pallas kernels: 111 us -> 105 us
  local copies, waits for them, and re-layouts: 5.75 us -> 1.67 us
    pallas_call x1, Pallas kernels: 111 us -> 105 us  [body(): pl.pallas_call(functools.partial(chain_kernel, (n, m, width, length)), ou...]
    unnamed x3 -> x1, local copies, waits for them, and re-layouts: 4.48 us -> 1.67 us
    reshape x1 -> x0, local copies, waits for them, and re-layouts: 1.28 us -> none  [body(): final_gain.reshape(1, dl)]
where the time goes in v2:
time: 107 us
  Pallas kernels  105 us (98%)
  local copies, waits for them, and re-layouts  1.67 us (2%)
    pallas_call x1, Pallas kernels, body(): pl.pallas_call(functools.partial(chain_kernel, (n, m, width, length)), ou...  105 us

profile of v2, /device:TPU:0, one launch (start us, length us, event | category | flops | bytes accessed | tf_op | source)
XLA Modules:
  0.0 106.7 jit_solution(3171239562146508453)
XLA Ops:
  0.0 105.0 %shard_map.100 = bf16[128,1024]{1,0:T(8,128)(2,1)} custom-call(bf16[128,1024]{1,0:T(8,128)(2,1)} %bitcast.5, bf16[2,1024]{1,0:T(2,128)(2,1)} %ng.1, bf16[3,2,3072]{2,1,0:T(2,128)(2,1)} %bitcast.6, bf16[3,2,3072]{2,1,0:T(2,128)(2,1)} %bitcast.7, bf16[2,3072]{1,0:T(2,128)(2,1)} %gb.1, bf16[2,3072]{1,0:T(2,128)(2,1)} %vb.1, bf16[1024]{0:T(1024)(128)(2,1)} %fg.1, ...), custom_call_target="tpu_custom_call" | custom-call | tf_op jit(solution)/shard_map/pallas_call | solution.py:328
  105.0 1.7 %copy.12 = bf16[2,64,1024]{2,1,0:T(8,128)(2,1)} copy(bf16[2,64,1024]{2,1,0:T(8,128)(2,1)} %bitcast.4) | data formatting | bytes 524288
